TPU v7x, 32 devices: a whole 2x2x4 slice. The times are simulated.
32 devices in a mesh: rep: 2 (over x), fs: 4 (over z), tp: 4 (over y, core).
Axes of the slice: x: 2, y: 2, z: 4, core: 2. Of those that a mesh axis runs over, the one named last changes fastest.
Arguments:
- tokens: bfloat16 [4096, 2048], P(('rep', 'fs', 'tp')), may hold values from -6 to 6
- mix_gain: bfloat16 [2048], replicated, may hold values from 0.099609375 to 1.8984375
- gate_proj: bfloat16 [2048, 512], P('fs', 'tp'), may hold values from -0.125 to 0.125
- value_proj: bfloat16 [2048, 512], P('fs', 'tp'), may hold values from -1 to 1
- layer_gain: bfloat16 [512], replicated, may hold values from 0.099609375 to 1.8984375
- layer_shift: bfloat16 [512], replicated, may hold values from -3 to 3
- mix_kernel: bfloat16 [4, 128, 128], replicated, may hold values from -0.5 to 0.5
- mix_offset: bfloat16 [4, 128], replicated, may hold values from -4 to 4
- out_proj: bfloat16 [2048, 512], P('fs', 'tp'), may hold values from -0.25 to 0.25
- ffn_gain: bfloat16 [2048], replicated, may hold values from 0.099609375 to 1.8984375
- ffn_gate: bfloat16 [2048, 5632], P('fs', 'tp'), may hold values from -0.125 to 0.125
- ffn_up: bfloat16 [2048, 5632], P('fs', 'tp'), may hold values from -0.125 to 0.125
- ffn_down: bfloat16 [2048, 5632], P('fs', 'tp'), may hold values from -0.078125 to 0.078125
Outputs:
- layer_out: bfloat16 [4096, 2048], P(('rep', 'fs', 'tp'))
All inputs are finite; a program needn't handle non-finite values.
Results may differ from a plain program's by a relative error of at most 0.015.
Values may be sent and summed in bfloat16 or wider, within the bound.
A program may use at most 64 MiB of HBM per device.

v0:
```python
import jax
import jax.numpy as jnp
from jax import lax
from jax.sharding import PartitionSpec as P

epsilon = 1e-06


def rms_norm(rows, gain):
    floats = rows.astype(jnp.float32)
    scale = lax.rsqrt(jnp.mean(floats * floats, axis=-1, keepdims=True) + epsilon)
    return (floats * scale * gain.astype(jnp.float32)).astype(jnp.bfloat16)


def contract_last(left, right):
    return lax.dot_general(
        left, right, (((1,), (1,)), ((), ())), preferred_element_type=jnp.float32
    )


def per_device(
    tokens,
    mix_gain,
    gate_proj,
    value_proj,
    layer_gain,
    layer_shift,
    mix_kernel,
    mix_offset,
    out_proj,
    ffn_gain,
    ffn_gate,
    ffn_up,
    ffn_down,
):
    normed = rms_norm(tokens, mix_gain)
    gate_rows, value_rows, out_rows = (
        lax.all_gather(gate_proj, "fs", axis=0, tiled=True),
        lax.all_gather(value_proj, "fs", axis=0, tiled=True),
        lax.all_gather(out_proj, "fs", axis=0, tiled=True),
    )
    mix_width = layer_gain.shape[0]
    groups = mix_kernel.shape[0]
    span_len = mix_kernel.shape[1]
    causal = jnp.tril(jnp.ones((span_len, span_len), dtype=bool))
    masked = jnp.where(causal[None], mix_kernel, jnp.zeros_like(mix_kernel))
    local_width = gate_rows.shape[1]
    first_col = lax.axis_index("tp") * local_width
    joined = jnp.concatenate([gate_rows, value_rows], axis=1)
    preact = jnp.dot(
        lax.all_gather(normed, "tp", axis=0, tiled=True), joined, preferred_element_type=jnp.float32
    )
    gate_u = jax.nn.gelu(preact[:, :local_width])
    activated = jax.nn.gelu(preact[:, local_width:])
    row_sum, squares = lax.psum(
        (jnp.sum(activated, axis=-1), jnp.sum(activated * activated, axis=-1)), "tp"
    )
    center = (row_sum / mix_width)[:, None]
    spread = (squares / mix_width)[:, None] - center * center
    gain_part = lax.dynamic_slice_in_dim(layer_gain, first_col, local_width).astype(jnp.float32)
    shift_part = lax.dynamic_slice_in_dim(layer_shift, first_col, local_width).astype(jnp.float32)
    values = ((activated - center) * lax.rsqrt(spread + epsilon) * gain_part + shift_part).astype(
        jnp.bfloat16
    )
    group_id = first_col // (mix_width // groups)
    kernel = lax.dynamic_index_in_dim(masked, group_id, 0, keepdims=False)
    offset = lax.dynamic_index_in_dim(mix_offset, group_id, 0, keepdims=False).astype(jnp.float32)
    mixing = jnp.einsum(
        "ts,nsc->ntc",
        kernel,
        values.reshape(-1, span_len, local_width),
        preferred_element_type=jnp.float32,
    )
    mixing = mixing + offset[None, :, None]
    gated_rows = (gate_u * mixing.reshape(gate_u.shape)).astype(jnp.bfloat16)
    mixer_out = lax.psum_scatter(
        contract_last(gated_rows, out_rows).astype(jnp.bfloat16),
        "tp",
        scatter_dimension=0,
        tiled=True,
    ).astype(jnp.float32)
    middle = (tokens.astype(jnp.float32) + mixer_out).astype(jnp.bfloat16)
    normed2 = rms_norm(middle, ffn_gain)
    gathered = lax.all_gather(normed2, "tp", axis=0, tiled=True)
    gate_pre = jnp.dot(
        gathered,
        lax.all_gather(ffn_gate, "fs", axis=0, tiled=True),
        preferred_element_type=jnp.float32,
    )
    up_pre = jnp.dot(
        gathered,
        lax.all_gather(ffn_up, "fs", axis=0, tiled=True),
        preferred_element_type=jnp.float32,
    )
    hidden = (jax.nn.silu(gate_pre) * up_pre).astype(jnp.bfloat16)
    partial_value = contract_last(hidden, lax.all_gather(ffn_down, "fs", axis=0, tiled=True))
    summed = lax.psum_scatter(
        partial_value.astype(jnp.bfloat16), "tp", scatter_dimension=0, tiled=True
    ).astype(jnp.float32)
    return (middle.astype(jnp.float32) + summed).astype(jnp.bfloat16)


def solution(mesh):
    placed = (
        P(("rep", "fs", "tp"), None),
        P(),
        P("fs", "tp"),
        P("fs", "tp"),
        P(),
        P(),
        P(),
        P(),
        P("fs", "tp"),
        P(),
        P("fs", "tp"),
        P("fs", "tp"),
        P("fs", "tp"),
    )
    return jax.shard_map(
        per_device,
        mesh=mesh,
        in_specs=placed,
        out_specs=P(("rep", "fs", "tp"), None),
        check_vma=False,
    )
```

profile of v0, /device:TPU:0, one launch (start us, length us, event | category | flops | bytes accessed | tf_op | source)
XLA Modules:
  0.0 472.7 jit_solution(3375747574779029369)
XLA Ops:
  7.4 0.7 convert_element_type.64
  8.1 1.2 fusion.1
  9.3 2.0 fusion.3
  11.5 0.7 bitcast_convert_fusion
  12.2 0.8 dynamic-slice_convert_fusion
  12.9 17.6 %all_gather.25 = bf16[2048,128]{1,0:T(8,128)(2,1)S(1)} all-gather(bf16[512,128]{1,0:T(8,128)(2,1)} %param.15), channel_id=1, replica_groups=mesh['rep'=2,'fs'=4,'tp'=4] {'fs'}, dimensions={0}, use_global_device_ids=true | all-gather | bytes 655360 | tf_op jit(solution)/shard_map/all_gather | solution.py:38
  30.5 16.7 %all_gather.26 = bf16[2048,128]{1,0:T(8,128)(2,1)S(1)} all-gather(bf16[512,128]{1,0:T(8,128)(2,1)S(1)} %copy-done.2), channel_id=1, replica_groups=mesh['rep'=2,'fs'=4,'tp'=4] {'fs'}, dimensions={0}, use_global_device_ids=true | all-gather | bytes 655360 | tf_op jit(solution)/shard_map/all_gather | solution.py:39
  47.2 15.6 %all_gather.27 = bf16[2048,128]{1,0:T(8,128)(2,1)S(1)} all-gather(bf16[512,128]{1,0:T(8,128)(2,1)S(1)} %copy-done.3), channel_id=1, replica_groups=mesh['rep'=2,'fs'=4,'tp'=4] {'fs'}, dimensions={0}, use_global_device_ids=true | all-gather | bytes 655360 | tf_op jit(solution)/shard_map/all_gather | solution.py:40
  62.8 2.3 fusion.9
  65.4 5.7 %all-reduce = (f32[512]{0:T(512)S(1)}, f32[512]{0:T(512)S(1)}) all-reduce(f32[512]{0:T(512)S(1)} %get-tuple-element.6, f32[512]{0:T(512)S(1)} %get-tuple-element.5), channel_id=1, replica_groups=mesh['rep'=2,'fs'=4,'tp'=4] {'tp'}, use_global_device_ids=true, to_apply=%region_4.5 | all-reduce | flops 1024 | bytes 8192 | tf_op jit(solution)/shard_map/psum | solution.py:55
  71.3 0.9 convolution_add_fusion
  72.4 2.1 convolution_convert_fusion
  75.1 31.4 %reduce-scatter.3.cloned.1.call-done = bf16[128,2048]{1,0:T(8,128)(2,1)} async-done(((bf16[512,2048]{1,0:T(8,128)(2,1)}), bf16[128,2048]{1,0:T(8,128)(2,1)}) %reduce-scatter.3.cloned.1.call-update) | async-done | bytes 524304 | tf_op jit(solution)/shard_map/reduce_scatter | solution.py:76
  106.5 1.3 fusion.5
  107.8 2.0 fusion.7
  110.6 0.7 all-gather.14.cloned.1.call-update
  111.3 72.6 %all-gather.10.cloned.1.call-done = bf16[2048,1408]{1,0:T(8,128)(2,1)} async-done(((bf16[512,1408]{1,0:T(8,128)(2,1)}), bf16[2048,1408]{1,0:T(8,128)(2,1)}) %all-gather.10.cloned.1.call-update) | async-done | bytes 5767184 | tf_op jit(solution)/shard_map/all_gather | solution.py:87
  183.9 22.1 %all-gather.8.cloned.1.call-done = bf16[512,2048]{1,0:T(8,128)(2,1)} async-done(((bf16[128,2048]{1,0:T(8,128)(2,1)}), bf16[512,2048]{1,0:T(8,128)(2,1)}) %all-gather.8.cloned.1.call-update) | async-done | bytes 2097168 | tf_op jit(solution)/shard_map/all_gather | solution.py:84
  206.0 8.4 %fusion.38 = f32[512,1408]{1,0:T(8,128)} fusion(bf16[512,2048]{1,0:T(8,128)(2,1)} %all-gather.8.cloned.1.call-done, bf16[2048,1408]{1,0:T(8,128)(2,1)} %all-gather.10.cloned.1.call-done), kind=kOutput, calls=%fused_computation.60 | convolution fusion | flops 2952790016 | bytes 10747904 | tf_op jit(solution)/shard_map/dot_general | solution.py:85
  214.4 99.6 %all-gather.12.cloned.1.call-done = bf16[2048,1408]{1,0:T(8,128)(2,1)} async-done(((bf16[512,1408]{1,0:T(8,128)(2,1)}), bf16[2048,1408]{1,0:T(8,128)(2,1)}) %all-gather.12.cloned.1.call-update) | async-done | bytes 5767184 | tf_op jit(solution)/shard_map/all_gather | solution.py:92
  314.0 106.4 %all-gather.14.cloned.1.call-done = bf16[2048,1408]{1,0:T(8,128)(2,1)} async-done(((bf16[512,1408]{1,0:T(8,128)(2,1)}), bf16[2048,1408]{1,0:T(8,128)(2,1)}) %all-gather.14.cloned.1.call-update) | async-done | bytes 5767184 | tf_op jit(solution)/shard_map/all_gather | solution.py:96
  420.5 13.2 %convolution_convert_fusion.1 = bf16[512,2048]{1,0:T(8,128)(2,1)} fusion(bf16[2048,1408]{1,0:T(8,128)(2,1)} %all-gather.14.cloned.1.call-done, bf16[512,2048]{1,0:T(8,128)(2,1)S(1)} %copy-done.5, bf16[2048,1408]{1,0:T(8,128)(2,1)} %all-gather.12.cloned.1.call-done, f32[512,1408]{1,0:T(8,128)} %fusion.38), kind=kOutput, calls=%fused_computation.3 | convolution fusion | flops 5910953984 | bytes 18612224 | tf_op jit(solution)/shard_map/dot_general | solution.py:16
  433.7 29.6 %reduce-scatter.5.cloned.1.call-done = bf16[128,2048]{1,0:T(8,128)(2,1)} async-done(((bf16[512,2048]{1,0:T(8,128)(2,1)}), bf16[128,2048]{1,0:T(8,128)(2,1)}) %reduce-scatter.5.cloned.1.call-update) | async-done | bytes 524304 | tf_op jit(solution)/shard_map/reduce_scatter | solution.py:97
  463.3 2.1 fusion.8
  (34 shorter events, 2.0 us)
Async XLA Ops:
  7.4 23.2 %copy-start.2 = (bf16[512,128]{1,0:T(8,128)(2,1)S(1)}, bf16[512,128]{1,0:T(8,128)(2,1)}, u32[]{:S(2)}) copy-start(bf16[512,128]{1,0:T(8,128)(2,1)} %param.16) | copy-start | bytes 393220
  7.4 39.9 %copy-start.3 = (bf16[512,128]{1,0:T(8,128)(2,1)S(1)}, bf16[512,128]{1,0:T(8,128)(2,1)}, u32[]{:S(2)}) copy-start(bf16[512,128]{1,0:T(8,128)(2,1)} %param.21) | copy-start | bytes 393220
  7.4 55.5 %all-gather.6.cloned.1.call-start = ((), (), s32[]{:S(2)}) async-start(), calls=%async_computation.2 | async-start | bytes 2621440 | tf_op jit(solution)/shard_map/all_gather | solution.py:51
  11.4 95.1 %reduce-scatter.3.cloned.1.call-start = ((), (), s32[]{:S(2)}) async-start(), calls=%async_computation.3 | async-start | bytes 2621440 | tf_op jit(solution)/shard_map/reduce_scatter | solution.py:76
  72.3 2.7 copy-start.4
  72.4 34.2 %copy-start = (bf16[128,2048]{1,0:T(8,128)(2,1)S(1)}, bf16[128,2048]{1,0:T(8,128)(2,1)}, u32[]{:S(2)}) copy-start(bf16[128,2048]{1,0:T(8,128)(2,1)} %param.13) | copy-start | bytes 1572868
  74.5 109.4 %all-gather.10.cloned.1.call-start = ((), (), s32[]{:S(2)}) async-start(), calls=%async_computation.5 | async-start | bytes 7208960 | tf_op jit(solution)/shard_map/all_gather | solution.py:87
  75.0 131.0 %all-gather.8.cloned.1.call-start = ((), (), s32[]{:S(2)}) async-start(), calls=%async_computation.4 | async-start | bytes 2621440 | tf_op jit(solution)/shard_map/all_gather | solution.py:84
  109.9 204.1 %all-gather.12.cloned.1.call-start = ((), (), s32[]{:S(2)}) async-start(), calls=%async_computation.6 | async-start | bytes 7208960 | tf_op jit(solution)/shard_map/all_gather | solution.py:92
  110.5 310.0 %all-gather.14.cloned.1.call-start = ((), (), s32[]{:S(2)}) async-start(), calls=%async_computation.7 | async-start | bytes 7208960 | tf_op jit(solution)/shard_map/all_gather | solution.py:96
  111.2 352.1 %reduce-scatter.5.cloned.1.call-start = ((), (), s32[]{:S(2)}) async-start(), calls=%async_computation.8 | async-start | bytes 2621440 | tf_op jit(solution)/shard_map/reduce_scatter | solution.py:97
  206.0 214.5 %copy-start.5 = (bf16[512,2048]{1,0:T(8,128)(2,1)S(1)}, bf16[512,2048]{1,0:T(8,128)(2,1)}, u32[]{:S(2)}) copy-start(bf16[512,2048]{1,0:T(8,128)(2,1)} %all-gather.8.cloned.1.call-done) | copy-start | bytes 6291460
  214.4 248.9 %copy-start.1 = (bf16[128,2048]{1,0:T(8,128)(2,1)S(1)}, bf16[128,2048]{1,0:T(8,128)(2,1)}, u32[]{:S(2)}) copy-start(bf16[128,2048]{1,0:T(8,128)(2,1)} %reduce-scatter.3.cloned.1.call-done) | copy-start | bytes 1572868
Sparse Core Ops, SparseCore 0:
  11.5 25.2 all-gather.5
  74.6 31.9 reduce-scatter.2
  433.8 29.4 reduce-scatter.4
Sparse Core Ops, SparseCore 1:
  76.5 107.3 all-gather.9
  185.3 20.7 all-gather.7
  207.5 106.5 all-gather.11
  315.6 104.8 all-gather.13
where the time goes:
time: 473 us
  waiting for transfers between devices  364 us (77%)
  blocking collectives  55.5 us (12%)
  matrix products  26.9 us (6%)
  between operations  14.9 us (3%)
  other arithmetic  11.5 us (2%)
    all_gather x1, waiting for transfers between devices, per_device(): lax.all_gather(ffn_down, 'fs', axis=0, tiled=True)  106 us
    all_gather x1, waiting for transfers between devices, per_device(): lax.all_gather(ffn_up, 'fs', axis=0, tiled=True)  99.6 us
    all_gather x1, waiting for transfers between devices, per_device(): lax.all_gather(ffn_gate, 'fs', axis=0, tiled=True)  72.6 us
    reduce_scatter x1, waiting for transfers between devices, per_device(): lax.psum_scatter(contract_last(gated_rows, out_rows).astype(jnp.bfloat16)...  31.4 us
    reduce_scatter x1, waiting for transfers between devices, per_device(): lax.psum_scatter(partial_value.astype(jnp.bfloat16), 'tp', scatter_dimens...  29.6 us
    all_gather x1, waiting for transfers between devices, per_device(): gathered = lax.all_gather(normed2, 'tp', axis=0, tiled=True)  22.1 us
    all_gather x1, blocking collectives, per_device(): lax.all_gather(gate_proj, 'fs', axis=0, tiled=True)  17.6 us
    all_gather x1, blocking collectives, per_device(): lax.all_gather(value_proj, 'fs', axis=0, tiled=True)  16.7 us
  transfers between devices with their start and end apart: 7, of which 6 were waited for; matrix products, arithmetic and copies ran while one was open for 3% of the time, Pallas kernels for 0%

commit v1 on v0

--- a/solution.py
+++ b/solution.py
@@ -4,6 +4,28 @@
 from jax.sharding import PartitionSpec as P
 
 epsilon = 1e-06
+
+
+def in_order(blocks, dim):
+    blocks = jnp.moveaxis(blocks, 0, dim)
+    lengths = blocks.shape
+    return blocks.reshape(*lengths[:dim], lengths[dim] * lengths[dim + 1], *lengths[dim + 2 :])
+
+
+def grow_blocks(x, axis):
+    size = lax.axis_size(axis)
+    blocks = x[None]
+    for level in range(size.bit_length() - 1):
+        apart = 1 << level
+        other = lax.ppermute(blocks, axis, [(i, i ^ apart) for i in range(size)])
+        both = jnp.stack([blocks, other])
+        upper = lax.axis_index(axis) >> level & 1
+        blocks = jnp.where(upper == 0, both, both[::-1]).reshape(-1, *x.shape)
+    return blocks
+
+
+def gather_by_bits(value, axis, dim):
+    return in_order(grow_blocks(value, axis), dim)
 
 
 def rms_norm(rows, gain):
@@ -93,7 +115,7 @@
         preferred_element_type=jnp.float32,
     )
     hidden = (jax.nn.silu(gate_pre) * up_pre).astype(jnp.bfloat16)
-    partial_value = contract_last(hidden, lax.all_gather(ffn_down, "fs", axis=0, tiled=True))
+    partial_value = contract_last(hidden, gather_by_bits(ffn_down, "fs", 0))
     summed = lax.psum_scatter(
         partial_value.astype(jnp.bfloat16), "tp", scatter_dimension=0, tiled=True
     ).astype(jnp.float32)

time: 473 us -> 501 us (1.059)
  waiting for transfers between devices: 364 us -> 380 us
  other arithmetic: 11.5 us -> 20 us
    ppermute x0 -> x2, waiting for transfers between devices: none -> 317 us  [grow_blocks(): other = lax.ppermute(blocks, axis, [(i, i ^ apart) for i in range(size)])]
    all_gather x1 -> x0, waiting for transfers between devices: 106 us -> none  [per_device(): lax.all_gather(ffn_down, 'fs', axis=0, tiled=True)]
    all_gather x1, waiting for transfers between devices: 99.6 us -> 0.01 us  [per_device(): lax.all_gather(ffn_up, 'fs', axis=0, tiled=True)]
    all_gather x1, waiting for transfers between devices: 72.6 us -> 0.01 us  [per_device(): lax.all_gather(ffn_gate, 'fs', axis=0, tiled=True)]
    all_gather x1, waiting for transfers between devices: 22.1 us -> 0.01 us  [per_device(): gathered = lax.all_gather(normed2, 'tp', axis=0, tiled=True)]
  transfers between devices with their start and end apart: 7 -> 8, of which waited for: 6 -> 4; matrix products, arithmetic and copies ran while one was open for 3% -> 4% of each run, Pallas kernels for 0% -> 0%
where the time goes in v1:
time: 501 us
  waiting for transfers between devices  380 us (76%)
  blocking collectives  55.5 us (11%)
  matrix products  26.9 us (5%)
  other arithmetic  20 us (4%)
  between operations  14.9 us (3%)
    ppermute x2, waiting for transfers between devices, grow_blocks(): other = lax.ppermute(blocks, axis, [(i, i ^ apart) for i in range(size)])  317 us
    reduce_scatter x1, waiting for transfers between devices, per_device(): lax.psum_scatter(contract_last(gated_rows, out_rows).astype(jnp.bfloat16)...  31.4 us
    reduce_scatter x1, waiting for transfers between devices, per_device(): lax.psum_scatter(partial_value.astype(jnp.bfloat16), 'tp', scatter_dimens...  30.4 us
    all_gather x1, blocking collectives, per_device(): lax.all_gather(gate_proj, 'fs', axis=0, tiled=True)  17.6 us
    all_gather x1, blocking collectives, per_device(): lax.all_gather(value_proj, 'fs', axis=0, tiled=True)  16.7 us
    all_gather x1, blocking collectives, per_device(): lax.all_gather(out_proj, 'fs', axis=0, tiled=True)  15.6 us
    dot_general x2, matrix products, contract_last(): lax.dot_general(left, right, (((1,), (1,)), ((), ())), preferred_element_...  15.3 us
  transfers between devices with their start and end apart: 8, of which 4 were waited for; matrix products, arithmetic and copies ran while one was open for 4% of the time, Pallas kernels for 0%

profile of v1, /device:TPU:0, one launch (start us, length us, event | category | flops | bytes accessed | tf_op | source)
XLA Modules:
  0.0 500.6 jit_solution(4833336444624557414)
XLA Ops:
  8.1 1.2 fusion.3
  9.3 2.0 fusion.5
  12.2 0.8 dynamic-slice_convert_fusion
  12.9 17.6 %all_gather.22 = bf16[2048,128]{1,0:T(8,128)(2,1)S(1)} all-gather(bf16[512,128]{1,0:T(8,128)(2,1)} %param.15), channel_id=1, replica_groups=mesh['rep'=2,'fs'=4,'tp'=4] {'fs'}, dimensions={0}, use_global_device_ids=true | all-gather | bytes 655360 | tf_op jit(solution)/shard_map/all_gather | solution.py:60
  30.5 16.7 %all_gather.23 = bf16[2048,128]{1,0:T(8,128)(2,1)S(1)} all-gather(bf16[512,128]{1,0:T(8,128)(2,1)S(1)} %copy-done.3), channel_id=1, replica_groups=mesh['rep'=2,'fs'=4,'tp'=4] {'fs'}, dimensions={0}, use_global_device_ids=true | all-gather | bytes 655360 | tf_op jit(solution)/shard_map/all_gather | solution.py:61
  47.2 15.6 %all_gather.24 = bf16[2048,128]{1,0:T(8,128)(2,1)S(1)} all-gather(bf16[512,128]{1,0:T(8,128)(2,1)S(1)} %copy-done.4), channel_id=1, replica_groups=mesh['rep'=2,'fs'=4,'tp'=4] {'fs'}, dimensions={0}, use_global_device_ids=true | all-gather | bytes 655360 | tf_op jit(solution)/shard_map/all_gather | solution.py:62
  62.8 2.3 fusion.11
  65.4 5.7 %all-reduce = (f32[512]{0:T(512)S(1)}, f32[512]{0:T(512)S(1)}) all-reduce(f32[512]{0:T(512)S(1)} %get-tuple-element.6, f32[512]{0:T(512)S(1)} %get-tuple-element.5), channel_id=1, replica_groups=mesh['rep'=2,'fs'=4,'tp'=4] {'tp'}, use_global_device_ids=true, to_apply=%region_4.5 | all-reduce | flops 1024 | bytes 8192 | tf_op jit(solution)/shard_map/psum | solution.py:77
  71.3 0.9 convolution_add_fusion
  72.4 2.0 convolution_convert_fusion
  75.1 31.4 %reduce-scatter.3.cloned.1.call-done = bf16[128,2048]{1,0:T(8,128)(2,1)} async-done(((bf16[512,2048]{1,0:T(8,128)(2,1)}), bf16[128,2048]{1,0:T(8,128)(2,1)}) %reduce-scatter.3.cloned.1.call-update) | async-done | bytes 524304 | tf_op jit(solution)/shard_map/reduce_scatter | solution.py:98
  106.5 1.3 fusion.7
  107.8 2.0 fusion.9
  110.7 1.6 collective-permute-start
  112.3 98.4 %collective-permute-done = bf16[1,512,1408]{2,1,0:T(8,128)(2,1)S(1)} collective-permute-done((bf16[1,512,1408]{2,1,0:T(8,128)(2,1)S(1)}, bf16[1,512,1408]{2,1,0:T(8,128)(2,1)S(1)}, u32[]{:S(2)}, u32[]{:S(2)}) %collective-permute-start) | collective-permute-done | bytes 1441824 | tf_op jit(solution)/shard_map/ppermute | solution.py:20
  210.9 2.2 fusion.2
  213.2 1.0 collective-permute-start.1
  214.1 218.9 %collective-permute-done.1 = bf16[2,512,1408]{2,1,0:T(8,128)(2,1)} collective-permute-done((bf16[2,512,1408]{2,1,0:T(8,128)(2,1)}, bf16[2,512,1408]{2,1,0:T(8,128)(2,1)}, u32[]{:S(2)}, u32[]{:S(2)}) %collective-permute-start.1) | collective-permute-done | bytes 2883616 | tf_op jit(solution)/shard_map/ppermute | solution.py:20
  433.0 2.4 pad_maximum_fusion
  435.4 3.6 reverse_select_fusion
  439.1 8.4 %fusion.40 = f32[512,1408]{1,0:T(8,128)} fusion(bf16[512,2048]{1,0:T(8,128)(2,1)} %all-gather.7.cloned.1.call-done, bf16[2048,1408]{1,0:T(8,128)(2,1)} %all-gather.9.cloned.1.call-done), kind=kOutput, calls=%fused_computation.66 | convolution fusion | flops 2952790016 | bytes 10747904 | tf_op jit(solution)/shard_map/dot_general | solution.py:107
  447.5 13.3 %convolution_convert_fusion.1 = bf16[512,2048]{1,0:T(8,128)(2,1)} fusion(bf16[2048,1408]{1,0:T(8,128)(2,1)} %bitcast.30, bf16[512,2048]{1,0:T(8,128)(2,1)S(1)} %copy-done.6, bf16[2048,1408]{1,0:T(8,128)(2,1)} %all-gather.11.cloned.1.call-done, f32[512,1408]{1,0:T(8,128)} %fusion.40), kind=kOutput, calls=%fused_computation.6 | convolution fusion | flops 5910953984 | bytes 18612224 | tf_op jit(solution)/shard_map/dot_general | solution.py:38
  460.8 30.4 %reduce-scatter.5.cloned.1.call-done = bf16[128,2048]{1,0:T(8,128)(2,1)} async-done(((bf16[512,2048]{1,0:T(8,128)(2,1)}), bf16[128,2048]{1,0:T(8,128)(2,1)}) %reduce-scatter.5.cloned.1.call-update) | async-done | bytes 524304 | tf_op jit(solution)/shard_map/reduce_scatter | solution.py:119
  491.2 2.1 fusion.10
  (41 shorter events, 3.9 us)
Async XLA Ops:
  7.4 23.2 %copy-start.3 = (bf16[512,128]{1,0:T(8,128)(2,1)S(1)}, bf16[512,128]{1,0:T(8,128)(2,1)}, u32[]{:S(2)}) copy-start(bf16[512,128]{1,0:T(8,128)(2,1)} %param.16) | copy-start | bytes 393220
  7.4 39.9 %copy-start.4 = (bf16[512,128]{1,0:T(8,128)(2,1)S(1)}, bf16[512,128]{1,0:T(8,128)(2,1)}, u32[]{:S(2)}) copy-start(bf16[512,128]{1,0:T(8,128)(2,1)} %param.21) | copy-start | bytes 393220
  7.4 55.5 %all-gather.5.cloned.1.call-start = ((), (), s32[]{:S(2)}) async-start(), calls=%async_computation.2 | async-start | bytes 2621440 | tf_op jit(solution)/shard_map/all_gather | solution.py:73
  11.4 95.1 %reduce-scatter.3.cloned.1.call-start = ((), (), s32[]{:S(2)}) async-start(), calls=%async_computation.3 | async-start | bytes 2621440 | tf_op jit(solution)/shard_map/reduce_scatter | solution.py:98
  72.3 2.7 copy-start.5
  72.3 34.2 %copy-start = (bf16[128,2048]{1,0:T(8,128)(2,1)S(1)}, bf16[128,2048]{1,0:T(8,128)(2,1)}, u32[]{:S(2)}) copy-start(bf16[128,2048]{1,0:T(8,128)(2,1)} %param.13) | copy-start | bytes 1572868
  74.4 36.3 %copy-start.2 = (bf16[512,1408]{1,0:T(8,128)(2,1)S(1)}, bf16[512,1408]{1,0:T(8,128)(2,1)}, u32[]{:S(2)}) copy-start(bf16[512,1408]{1,0:T(8,128)(2,1)} %param.25) | copy-start | bytes 4325380
  74.4 364.7 %all-gather.9.cloned.1.call-start = ((), (), s32[]{:S(2)}) async-start(), calls=%async_computation.5 | async-start | bytes 7208960 | tf_op jit(solution)/shard_map/all_gather | solution.py:109
  75.0 364.1 %all-gather.7.cloned.1.call-start = ((), (), s32[]{:S(2)}) async-start(), calls=%async_computation.4 | async-start | bytes 2621440 | tf_op jit(solution)/shard_map/all_gather | solution.py:106
  109.9 337.6 %all-gather.11.cloned.1.call-start = ((), (), s32[]{:S(2)}) async-start(), calls=%async_computation.6 | async-start | bytes 7208960 | tf_op jit(solution)/shard_map/all_gather | solution.py:114
  110.5 380.7 %reduce-scatter.5.cloned.1.call-start = ((), (), s32[]{:S(2)}) async-start(), calls=%async_computation.7 | async-start | bytes 2621440 | tf_op jit(solution)/shard_map/reduce_scatter | solution.py:119
  110.7 99.9 %collective-permute-start = (bf16[1,512,1408]{2,1,0:T(8,128)(2,1)S(1)}, bf16[1,512,1408]{2,1,0:T(8,128)(2,1)S(1)}, u32[]{:S(2)}, u32[]{:S(2)}) collective-permute-start(bf16[1,512,1408]{2,1,0:T(8,128)(2,1)S(1)} %bitcast.31), channel_id=1, source_target_pairs={{0,4},{4,0},{8,12},{12,8},{1,5},{5,1},{9,13},{13,9},{2,6},{6,2},{1... | collective-permute-start | bytes 4325384 | tf_op jit(solution)/shard_map/ppermute | solution.py:20
  213.2 219.9 %collective-permute-start.1 = (bf16[2,512,1408]{2,1,0:T(8,128)(2,1)}, bf16[2,512,1408]{2,1,0:T(8,128)(2,1)}, u32[]{:S(2)}, u32[]{:S(2)}) collective-permute-start(bf16[2,512,1408]{2,1,0:T(8,128)(2,1)} %get-tuple-element.10), channel_id=1, source_target_pairs={{0,8},{4,12},{8,0},{12,4},{1,9},{5,13},{9,1},{13,5},{2,10},{6,14},... | collective-permute-start | bytes 8650760 | tf_op jit(solution)/shard_map/ppermute | solution.py:20
  439.1 8.4 %copy-start.6 = (bf16[512,2048]{1,0:T(8,128)(2,1)S(1)}, bf16[512,2048]{1,0:T(8,128)(2,1)}, u32[]{:S(2)}) copy-start(bf16[512,2048]{1,0:T(8,128)(2,1)} %all-gather.7.cloned.1.call-done) | copy-start | bytes 6291460
  447.5 43.7 %copy-start.1 = (bf16[128,2048]{1,0:T(8,128)(2,1)S(1)}, bf16[128,2048]{1,0:T(8,128)(2,1)}, u32[]{:S(2)}) copy-start(bf16[128,2048]{1,0:T(8,128)(2,1)} %reduce-scatter.3.cloned.1.call-done) | copy-start | bytes 1572868
Sparse Core Ops, SparseCore 0:
  11.5 25.2 all-gather.4
  74.5 31.9 reduce-scatter.2
  460.9 30.2 reduce-scatter.4
Sparse Core Ops, SparseCore 1:
  76.5 136.0 all-gather.8
  213.9 22.5 all-gather.6
  238.0 179.8 all-gather.10
